TPU v7x, 32 devices: a whole 2x2x4 slice. The times are simulated.
32 devices in a mesh: ep: 4 (over z), tp: 8 (over y, x, core).
Axes of the slice: x: 2, y: 2, z: 4, core: 2. Of those that a mesh axis runs over, the one named last changes fastest.
Arguments:
- tokens: bfloat16 [512, 2048], P('ep'), may hold values from -6 to 6
- norm_gain: float32 [2048], replicated, may hold values from 0.1 to 1.9
- route_ids: int32 [512, 2], P('ep'), may hold values from 0 to 3, all different within a row; in each aligned block of 128 rows (0 to 127, 128 to 255, ...) at most 96 rows name the same one
- route_weights: float32 [512, 2], P('ep'), may hold values from 0.05 to 1
- gate_proj: bfloat16 [4, 2048, 12288], P('ep', None, 'tp'), may hold values from -0.125 to 0.125
- up_proj: bfloat16 [4, 2048, 12288], P('ep', None, 'tp'), may hold values from -0.125 to 0.125
- down_proj: bfloat16 [4, 12288, 2048], P('ep', 'tp'), may hold values from -0.0546875 to 0.0546875
Outputs:
- mixed: bfloat16 [512, 2048], P('ep', 'tp')
Inputs may be any that keep to these rules, and one draw needn't show every extreme that they name: `route_ids`: each token names 2 different experts; within the rows of one device (aligned blocks of 128 tokens) no expert is named by more than 96 pairs, a bound that some block reaches.
All inputs are finite; a program needn't handle non-finite values.
Results may differ from a plain program's by a relative error of at most 0.017.
Values may be sent and summed in bfloat16 or wider, within the bound.
No kernel may reach another device: no remote copies, remote signals or barrier semaphores. Data moves between devices by JAX's collectives and lax.ppermute only.
A program may use at most 64 MiB of HBM per device.

v0:
```python
import jax
import jax.numpy as jnp
from jax import lax
from jax.sharding import PartitionSpec as P


def local(tokens, norm_gain, route_ids, route_weights, gate_proj, up_proj, down_proj):
    ep_count = lax.axis_size("ep")
    tp_count = lax.axis_size("tp")
    tok_rows, width = tokens.shape
    topk = route_ids.shape[1]
    capacity = min(tok_rows, (3 * tok_rows * topk + 2 * ep_count - 1) // (2 * ep_count))
    share_width = width // tp_count
    values = tokens.astype(jnp.float32)
    mean_square = jnp.mean(values * values, axis=-1, keepdims=True)
    normed = (values * lax.rsqrt(mean_square + 1e-06) * norm_gain).astype(jnp.bfloat16)
    route_flat = route_ids.reshape(-1)
    onehot = (route_flat[:, None] == jnp.arange(ep_count, dtype=jnp.int32)[None, :]).astype(
        jnp.int32
    )
    slot_index = jnp.sum((jnp.cumsum(onehot, axis=0) - onehot) * onehot, axis=1)
    repeated = jnp.repeat(normed, topk, axis=0)
    down_local = down_proj[0]
    outgoing = (
        jnp.zeros((ep_count, capacity, width), jnp.bfloat16)
        .at[route_flat, slot_index]
        .set(repeated)
    )
    arrived = lax.all_to_all(outgoing, "ep", split_axis=0, concat_axis=0, tiled=True)
    item_rows = arrived.shape[1]
    merged_rows = arrived.reshape(-1, width)
    gate_act = jnp.dot(merged_rows, gate_proj[0], preferred_element_type=jnp.float32)
    up_act = jnp.dot(merged_rows, up_proj[0], preferred_element_type=jnp.float32)
    hidden = (jax.nn.silu(gate_act) * up_act).astype(jnp.bfloat16)
    term = lax.dot_general(
        down_local, hidden, (((0,), (1,)), ((), ())), preferred_element_type=jnp.float32
    )
    term = lax.optimization_barrier(term.astype(jnp.bfloat16))
    summed = lax.psum_scatter(
        term.astype(jnp.float32).astype(jnp.bfloat16), "tp", scatter_dimension=0, tiled=True
    ).astype(jnp.float32)
    back = summed.T.reshape(ep_count, item_rows, share_width)
    returned = lax.all_to_all(
        back.astype(jnp.bfloat16), "ep", split_axis=0, concat_axis=0, tiled=True
    ).astype(back.dtype)
    columns_back = returned.shape[2]
    picked = returned[route_flat, slot_index].reshape(tok_rows, topk, columns_back)
    weighted = jnp.sum(route_weights[:, :, None] * picked, axis=1)
    return weighted.astype(jnp.bfloat16)


def solution(mesh):
    placed = (
        P("ep", None),
        P(),
        P("ep", None),
        P("ep", None),
        P("ep", None, "tp"),
        P("ep", None, "tp"),
        P("ep", "tp", None),
    )
    return jax.shard_map(
        local, mesh=mesh, in_specs=placed, out_specs=P("ep", "tp"), check_vma=False
    )
```

profile of v0, /device:TPU:0, one launch (start us, length us, event | category | flops | bytes accessed | tf_op | source)
XLA Modules:
  0.0 157.4 jit_solution(11334594695858422979)
XLA Ops:
  6.5 0.0 reduce-scatter.2.cloned.1.call-start
  6.5 0.8 copy.12
  7.3 0.1 eq.29
  7.5 0.1 eq.25
  7.6 0.1 reshape.82
  7.8 1.2 reduce-window.6
  9.0 0.1 slice.12
  9.1 0.1 copy.15
  9.2 0.1 copy.16
  9.3 0.1 add_bitcast_fusion
  9.4 1.2 fusion.18
  10.6 1.2 fusion.20
  11.9 0.6 broadcast_in_dim.5
  12.5 0.4 reshape.95
  13.0 0.2 broadcast_in_dim.4
  13.2 23.1 %scatter_fusion = bf16[4,96,2048]{2,1,0:T(8,128)(2,1)S(1)} fusion(bf16[4,96,2048]{2,1,0:T(8,128)(2,1)S(1)} %broadcast_in_dim.4, s32[256]{0:T(256)S(1)} %bitcast.49, bf16[256,2048]{1,0:T(8,128)(2,1)S(1)} %reshape.95), kind=kCustom, calls=%fused_computation.1 | custom fusion | bytes 3147776 | tf_op jit(solution)/shard_map/scatter | solution.py:27
  36.3 43.1 %all_to_all.10 = bf16[4,96,2048]{2,1,0:T(8,128)(2,1)S(1)} all-to-all(bf16[4,96,2048]{2,1,0:T(8,128)(2,1)S(1)} %scatter_fusion), channel_id=1, replica_groups=mesh['ep'=4,'tp'=8] {'ep'}, dimensions={0} | all-to-all | bytes 3145728 | tf_op jit(solution)/shard_map/all_to_all | solution.py:29
  79.4 6.8 %fusion.4 = f32[384,1536]{1,0:T(8,128)} fusion(bf16[384,2048]{1,0:T(8,128)(2,1)S(1)} %bitcast.51, bf16[1,2048,1536]{2,1,0:T(8,128)(2,1)} %param.11), kind=kOutput, calls=%fused_computation.6 | convolution fusion | flops 2415919104 | bytes 10223616 | tf_op jit(solution)/shard_map/dot_general | solution.py:32
  86.2 0.0 copy-start
  86.2 11.6 %fusion.15 = bf16[2048,384]{0,1:T(8,128)(2,1)} fusion(bf16[1,1536,2048]{2,1,0:T(8,128)(2,1)} %param.13, bf16[384,2048]{1,0:T(8,128)(2,1)S(1)} %bitcast.52, bf16[1,2048,1536]{2,1,0:T(8,128)(2,1)} %param.12, f32[384,1536]{1,0:T(8,128)} %fusion.4), kind=kOutput, calls=%fused_computation.11 | convolution fusion | flops 4836163584 | bytes 18087936 | tf_op jit(solution)/shard_map/dot_general | solution.py:35
  97.8 0.0 reduce-scatter.2.cloned.1.call-update
  97.8 37.6 %reduce-scatter.2.cloned.1.call-done = bf16[256,384]{0,1:T(8,128)(2,1)} async-done(((bf16[2048,384]{0,1:T(8,128)(2,1)}), bf16[256,384]{0,1:T(8,128)(2,1)}) %reduce-scatter.2.cloned.1.call-update) | async-done | bytes 196624 | tf_op jit(solution)/shard_map/reduce_scatter | solution.py:39
  135.4 4.6 %all-to-all-start.1 = ((bf16[4,96,256]{2,1,0:T(8,128)(2,1)}), bf16[4,96,256]{2,1,0:T(8,128)(2,1)S(1)}, u32[]{:S(2)}, u32[]{:S(2)}) async-start(bf16[4,96,256]{2,1,0:T(8,128)(2,1)} %bitcast.53), calls=%async_computation.2 | async-start | bytes 393216 | tf_op jit(solution)/shard_map/all_to_all | solution.py:43
  140.0 0.0 copy-done
  140.0 0.1 copy.11
  140.2 7.2 %all-to-all-done.1 = bf16[4,96,256]{2,1,0:T(8,128)(2,1)S(1)} async-done(((bf16[4,96,256]{2,1,0:T(8,128)(2,1)}), bf16[4,96,256]{2,1,0:T(8,128)(2,1)S(1)}, u32[]{:S(2)}, u32[]{:S(2)}) %all-to-all-start.1) | async-done | bytes 196640 | tf_op jit(solution)/shard_map/all_to_all | solution.py:43
  147.4 2.0 %gather_fusion = f32[256,256]{1,0:T(8,128)S(1)} fusion(f32[4,96,256]{2,1,0:T(8,128)S(1)} %convert_element_type.47, s32[256]{0:T(256)S(1)} %bitcast.50), kind=kCustom, calls=%fused_computation | custom fusion | bytes 526336 | tf_op jit(solution)/shard_map/gather | solution.py:47
  149.4 0.1 reshape.86
  149.5 1.0 multiply_reduce_fusion
  (7 shorter events, 0.1 us)
Async XLA Ops:
  6.5 128.9 %reduce-scatter.2.cloned.1.call-start = ((), (), s32[]{:S(2)}) async-start(), calls=%async_computation.3 | async-start | bytes 1769472 | tf_op jit(solution)/shard_map/reduce_scatter | solution.py:39
  86.2 53.9 %copy-start = (f32[128,2]{0,1:T(2,128)S(1)}, f32[128,2]{0,1:T(2,128)}, u32[]{:S(2)}) copy-start(f32[128,2]{0,1:T(2,128)} %param.10) | copy-start | bytes 3076
  135.4 11.9 %all-to-all-start.1 = ((bf16[4,96,256]{2,1,0:T(8,128)(2,1)}), bf16[4,96,256]{2,1,0:T(8,128)(2,1)S(1)}, u32[]{:S(2)}, u32[]{:S(2)}) async-start(bf16[4,96,256]{2,1,0:T(8,128)(2,1)} %bitcast.53), calls=%async_computation.2 | async-start | bytes 393216 | tf_op jit(solution)/shard_map/all_to_all | solution.py:43
Sparse Core Ops, SparseCore 0:
  98.0 37.4 reduce-scatter.1
where the time goes:
time: 158 us; the launch traced here: 157 us
  waiting for transfers between devices  44.8 us (28%)
  blocking collectives  43.1 us (27%)
  local copies, waits for them, and re-layouts  28.1 us (18%)
  matrix products  18.4 us (12%)
  between operations  13.5 us (9%)
  other arithmetic  4.92 us (3%)
  starting transfers between devices  4.61 us (3%)
    all_to_all x1, blocking collectives, local(): lax.all_to_all(outgoing, 'ep', split_axis=0, concat_axis=0, tiled=True)  43.1 us
    reduce_scatter x1, waiting for transfers between devices, local(): lax.psum_scatter(term.astype(jnp.float32).astype(jnp.bfloat16), 'tp', sca...  37.6 us
    scatter x1, local copies, waits for them, and re-layouts, local(): outgoing = jnp.zeros((ep_count, capacity, width), jnp.bfloat16).at[route_...  23.1 us
    dot_general x1, matrix products, local(): lax.dot_general(down_local, hidden, (((0,), (1,)), ((), ())), preferred_e...  11.6 us
    all_to_all x1, waiting for transfers between devices, local(): lax.all_to_all(back.astype(jnp.bfloat16), 'ep', split_axis=0, concat_axis...  7.19 us
    dot_general x1, matrix products, local(): jnp.dot(merged_rows, gate_proj[0], preferred_element_type=jnp.float32)  6.79 us
    all_to_all x1, starting transfers between devices, local(): lax.all_to_all(back.astype(jnp.bfloat16), 'ep', split_axis=0, concat_axis...  4.61 us
  transfers between devices with their start and end apart: 2, of which 2 were waited for; matrix products, arithmetic and copies ran while one was open for 0% of the time, Pallas kernels for 0%

commit v1 on v0

v1 whole, which is shorter than its diff:
```python
import jax
import jax.numpy as jnp
from jax import lax
from jax.experimental import pallas as pl
from jax.experimental.pallas import tpu as pltpu
from jax.sharding import PartitionSpec as P


def steps_below(position, size, count):
    total = jnp.zeros_like(position)
    for step in range(1, count):
        total = total + (position >= step * size).astype(jnp.int32)
    return total


def selection(ids, expert, slot, first, second):
    rows = ids.shape[0]
    hit0 = ids[:, 0:1] == expert
    hit1 = ids[:, 1:2] == expert
    member = jnp.where(hit0 | hit1, 1.0, 0.0).astype(jnp.bfloat16)
    earlier = (
        lax.broadcasted_iota(jnp.int32, (rows, rows), 1)
        < lax.broadcasted_iota(jnp.int32, (rows, rows), 0)
    )
    earlier = jnp.where(earlier, 1.0, 0.0).astype(jnp.bfloat16)
    place = jnp.dot(earlier, member, preferred_element_type=jnp.float32)
    here = place == slot.astype(jnp.float32)
    return jnp.where(here & hit0, first, 0.0) + jnp.where(here & hit1, second, 0.0)


def dispatch_kernel(where_ref, tokens_ref, gain_ref, ids_ref, weights_ref, *outs, ep, cap):
    half = cap // 2
    mix_ref, own_ref, sends = outs[0], outs[1], outs[2:]
    mine = where_ref[0]
    core = where_ref[1]
    values = tokens_ref[...].astype(jnp.float32)
    mean_square = jnp.mean(values * values, axis=-1, keepdims=True)
    normed = (values * lax.rsqrt(mean_square + 1e-06) * gain_ref[...]).astype(jnp.bfloat16)
    ids = ids_ref[...]
    weights = weights_ref[...]
    rows = ids.shape[0]

    lanes = cap + (ep - 1) * half
    lane = lax.broadcasted_iota(jnp.int32, (rows, lanes), 1)
    rest = lane - cap
    away = jnp.where(lane < cap, 0, 1 + steps_below(rest, half, ep - 1))
    slot = jnp.where(lane < cap, lane, rest - (away - 1) * half + core * half)
    expert = mine + away
    expert = jnp.where(expert >= ep, expert - ep, expert)
    chosen = selection(ids, expert, slot, 1.0, 1.0).astype(jnp.bfloat16)
    picked = lax.dot_general(
        chosen, normed, (((0,), (0,)), ((), ())), preferred_element_type=jnp.float32
    ).astype(jnp.bfloat16)
    own_ref[...] = picked[:cap]
    for at, send_ref in enumerate(sends):
        send_ref[...] = picked[cap + at * half : cap + (at + 1) * half]

    lane = lax.broadcasted_iota(jnp.int32, (rows, ep * cap), 1)
    away = steps_below(lane, cap, ep)
    expert = mine + away
    expert = jnp.where(expert >= ep, expert - ep, expert)
    mix_ref[...] = selection(ids, expert, lane - away * cap, weights[:, 0:1], weights[:, 1:2])


def down_kernel(where_ref, hidden_ref, down_ref, out_ref):
    out_ref[0] = jnp.dot(
        hidden_ref[...], down_ref[...], preferred_element_type=jnp.float32
    ).astype(out_ref.dtype)


def down_blocks(hidden, down, parity, blocks):
    rows, inner = hidden.shape
    share = down.shape[1] // blocks
    if share % 128:
        whole = lax.dot_general(
            down, hidden, (((0,), (1,)), ((), ())), preferred_element_type=jnp.float32
        )
        whole = whole.astype(jnp.bfloat16).reshape(blocks // 2, 2, share, rows)
        return jnp.swapaxes(lax.dynamic_index_in_dim(whole, parity, 1, keepdims=False), 1, 2)
    return pl.pallas_call(
        down_kernel,
        out_shape=jax.ShapeDtypeStruct((blocks // 2, rows, share), jnp.bfloat16),
        grid_spec=pltpu.PrefetchScalarGridSpec(
            num_scalar_prefetch=1,
            grid=(blocks // 2,),
            in_specs=[
                pl.BlockSpec((rows, inner), lambda i, where: (0, 0)),
                pl.BlockSpec((inner, share), lambda i, where: (0, 2 * i + where[0])),
            ],
            out_specs=pl.BlockSpec((1, rows, share), lambda i, where: (i, 0, 0)),
        ),
        compiler_params=pltpu.CompilerParams(dimension_semantics=("arbitrary",)),
        cost_estimate=pl.CostEstimate(
            flops=rows * inner * down.shape[1],
            bytes_accessed=inner * down.shape[1],
            transcendentals=0,
        ),
    )(parity.reshape(1), hidden, down)


def combine_kernel(mix_ref, *refs):
    out_ref, blocks = refs[-1], refs[:-1]
    cap = blocks[0].shape[0]
    total = None
    for at, block_ref in enumerate(blocks):
        mix = mix_ref[:, at * cap : (at + 1) * cap]
        high = mix.astype(jnp.bfloat16)
        low = (mix - high.astype(jnp.float32)).astype(jnp.bfloat16)
        block = block_ref[...]
        for piece in (high, low):
            term = jnp.dot(piece, block, preferred_element_type=jnp.float32)
            total = term if total is None else total + term
    out_ref[...] = total.astype(out_ref.dtype)


def local(tokens, norm_gain, route_ids, route_weights, gate_proj, up_proj, down_proj):
    ep = lax.axis_size("ep")
    tp = lax.axis_size("tp")
    rows, width = tokens.shape
    topk = route_ids.shape[1]
    cap = min(rows, (3 * rows * topk + 2 * ep - 1) // (2 * ep))
    half = cap // 2
    share = width // tp
    bits = tp.bit_length() - 1
    assert tp == 1 << bits and topk == 2
    at_ep = lax.axis_index("ep").astype(jnp.int32)
    at_tp = lax.axis_index("tp").astype(jnp.int32)
    core = at_tp & 1

    bf16 = jnp.bfloat16
    prepared = pl.pallas_call(
        lambda *refs: dispatch_kernel(*refs, ep=ep, cap=cap),
        out_shape=[
            jax.ShapeDtypeStruct((rows, ep * cap), jnp.float32),
            jax.ShapeDtypeStruct((cap, width), bf16),
        ]
        + [jax.ShapeDtypeStruct((half, width), bf16)] * (ep - 1),
        in_specs=[pl.BlockSpec(memory_space=pltpu.SMEM)]
        + [pl.BlockSpec(memory_space=pltpu.VMEM)] * 4,
    )(jnp.stack([at_ep, core]), tokens, norm_gain.reshape(1, width), route_ids, route_weights)
    mix, own, sends = prepared[0], prepared[1], prepared[2:]

    pairs = [(i, i ^ 1) for i in range(tp)]
    pieces = [own]
    for away, send in enumerate(sends, 1):
        got = lax.ppermute(send, "ep", [(i, (i + away) % ep) for i in range(ep)])
        other = lax.ppermute(got, "tp", pairs)
        pieces += [jnp.where(core == 0, got, other), jnp.where(core == 0, other, got)]
    merged = jnp.concatenate(pieces, axis=0)

    gate = jnp.dot(merged, gate_proj[0], preferred_element_type=jnp.float32)
    up = jnp.dot(merged, up_proj[0], preferred_element_type=jnp.float32)
    hidden = (jax.nn.silu(gate) * up).astype(bf16)

    send = down_blocks(hidden, down_proj[0], 1 - core, tp)
    got = lax.ppermute(send, "tp", pairs)
    keep = down_blocks(hidden, down_proj[0], core, tp)
    count = ep * cap
    total = keep.astype(jnp.float32) + got.astype(jnp.float32)
    total = total.reshape((2,) * (bits - 1) + (count, share))
    axes = tuple(range(bits - 2, -1, -1)) + (bits - 1, bits)
    total = jnp.where(core == 0, jnp.transpose(total, axes), total).astype(bf16)
    for step in range(bits - 1):
        even, odd = 1 + step, bits - 1 - step
        bit = jnp.where(core == 0, at_tp >> even, at_tp >> odd) & 1
        swap = [(i, i ^ (1 << (odd if i & 1 else even))) for i in range(tp)]
        send = lax.dynamic_index_in_dim(total, 1 - bit, 0, keepdims=False)
        keep = lax.dynamic_index_in_dim(total, bit, 0, keepdims=False)
        got = lax.ppermute(send, "tp", swap)
        total = (keep.astype(jnp.float32) + got.astype(jnp.float32)).astype(bf16)

    back = [total[:cap]]
    for away in range(1, ep):
        block = total[away * cap : (away + 1) * cap]
        back.append(lax.ppermute(block, "ep", [(i, (i - away) % ep) for i in range(ep)]))
    return pl.pallas_call(
        combine_kernel,
        out_shape=jax.ShapeDtypeStruct((rows, share), bf16),
        in_specs=[pl.BlockSpec(memory_space=pltpu.VMEM)] * (ep + 1),
    )(mix, *back)


def solution(mesh):
    placed = (
        P("ep", None),
        P(),
        P("ep", None),
        P("ep", None),
        P("ep", None, "tp"),
        P("ep", None, "tp"),
        P("ep", "tp", None),
    )
    return jax.shard_map(
        local, mesh=mesh, in_specs=placed, out_specs=P("ep", "tp"), check_vma=False
    )
```

time: 158 us -> 75.1 us (0.48)
  blocking collectives: 43.1 us -> 0 us
  local copies, waits for them, and re-layouts: 28.1 us -> 5.15 us
  waiting for transfers between devices: 44.8 us -> 25.4 us
  Pallas kernels: 0 us -> 14.8 us
  starting transfers between devices: 4.61 us -> 18 us
  between operations: 13.5 us -> 0.13 us
  matrix products: 18.4 us -> 8.67 us
  other arithmetic: 4.92 us -> 2.54 us
    all_to_all x1 -> x0, blocking collectives: 43.1 us -> none  [local(): lax.all_to_all(outgoing, 'ep', split_axis=0, concat_axis=0, tiled=True)]
    reduce_scatter x1 -> x0, waiting for transfers between devices: 37.6 us -> none  [local(): lax.psum_scatter(term.astype(jnp.float32).astype(jnp.bfloat16), 'tp', sca...]
    ppermute x0 -> x12, waiting for transfers between devices: none -> 25.4 us  [the longest x3 10.7 us: local(): got = lax.ppermute(send, 'ep', [(i, (i + away) % ep) for i in range(ep)])]
    scatter x1 -> x0, local copies, waits for them, and re-layouts: 23.1 us -> none  [local(): outgoing = jnp.zeros((ep_count, capacity, width), jnp.bfloat16).at[route_...]
    ppermute x0 -> x12, starting transfers between devices: none -> 18 us  [the longest x3 7.21 us: local(): lax.ppermute(block, 'ep', [(i, (i - away) % ep) for i in range(ep)])]
    pallas_call x0 -> x4, Pallas kernels: none -> 14.8 us  [the longest x2 10 us: down_blocks(): pl.pallas_call(down_kernel, out_shape=jax.ShapeDtypeStruct((blocks // 2,...]
    dot_general x2, matrix products: 18.4 us -> 8.67 us  [the longest x1 4.88 us: local(): gate = jnp.dot(merged, gate_proj[0], preferred_element_type=jnp.float32)]
    all_to_all x1 -> x0, waiting for transfers between devices: 7.19 us -> none  [local(): lax.all_to_all(back.astype(jnp.bfloat16), 'ep', split_axis=0, concat_axis...]
  transfers between devices with their start and end apart: 2 -> 12, of which waited for: 2 -> 8; matrix products, arithmetic and copies ran while one was open for 0% -> 2% of each run, Pallas kernels for 0% -> 7%
where the time goes in v1:
time: 75.1 us; the launch traced here: 74.6 us
  waiting for transfers between devices  25.4 us (34%)
  starting transfers between devices  18 us (24%)
  Pallas kernels  14.8 us (20%)
  matrix products  8.67 us (12%)
  local copies, waits for them, and re-layouts  5.15 us (7%)
  other arithmetic  2.54 us (3%)
    ppermute x3, waiting for transfers between devices, local(): got = lax.ppermute(send, 'ep', [(i, (i + away) % ep) for i in range(ep)])  10.7 us
    ppermute x2, waiting for transfers between devices, local(): got = lax.ppermute(send, 'tp', swap)  10.5 us
    pallas_call x2, Pallas kernels, down_blocks(): pl.pallas_call(down_kernel, out_shape=jax.ShapeDtypeStruct((blocks // 2,...  10 us
    ppermute x3, starting transfers between devices, local(): lax.ppermute(block, 'ep', [(i, (i - away) % ep) for i in range(ep)])  7.21 us
    ppermute x3, starting transfers between devices, local(): got = lax.ppermute(send, 'ep', [(i, (i + away) % ep) for i in range(ep)])  6.99 us
    dot_general x1, matrix products, local(): gate = jnp.dot(merged, gate_proj[0], preferred_element_type=jnp.float32)  4.88 us
    unnamed x13, local copies, waits for them, and re-layouts  4.47 us
    dot_general x1, matrix products, local(): up = jnp.dot(merged, up_proj[0], preferred_element_type=jnp.float32)  3.79 us
  transfers between devices with their start and end apart: 12, of which 8 were waited for; matrix products, arithmetic and copies ran while one was open for 2% of the time, Pallas kernels for 7%

profile of v1, /device:TPU:0, one launch (start us, length us, event | category | flops | bytes accessed | tf_op | source)
XLA Modules:
  0.0 74.6 jit_solution(14291820151920695927)
XLA Ops:
  0.0 1.4 %copy.8.refs_3_ = s32[128,2]{1,0:T(8,128)} copy(s32[128,2]{0,1:T(2,128)} %param.9) | data formatting | bytes 2048 | tf_op args[2]
  1.4 1.4 %copy.9.refs_4_ = f32[128,2]{1,0:T(8,128)} copy(f32[128,2]{0,1:T(2,128)} %param.10) | data formatting | bytes 2048 | tf_op args[3]
  2.8 0.7 pad_add_fusion.refs_0_
  3.5 2.8 %shard_map.73 = (f32[128,384]{1,0:T(8,128)}, bf16[96,2048]{1,0:T(8,128)(2,1)}, bf16[48,2048]{1,0:T(8,128)(2,1)}, bf16[48,2048]{1,0:T(8,128)(2,1)}, bf16[48,2048]{1,0:T(8,128)(2,1)}) custom-call(s32[2]{0:T(128)} %pad_add_fusion.refs_0_, bf16[128,2048]{1,0:T(8,128)(2,1)} %refs_1_.1, f32[1,2048]{1,0:T(1,128)} %bitcast.32, s32[128,2]{1,0:T(8,128)} %copy.8.refs_3_, ...), custom_call_target="tpu_custom_call" | custom-call | tf_op jit(solution)/shard_map/pallas_call | solution.py:131
  6.2 3.1 %collective-permute-start = (bf16[48,2048]{1,0:T(8,128)(2,1)}, bf16[48,2048]{1,0:T(8,128)(2,1)S(1)}, u32[]{:S(2)}, u32[]{:S(2)}) collective-permute-start(bf16[48,2048]{1,0:T(8,128)(2,1)} %get-tuple-element.12), channel_id=1, source_target_pairs={{0,8},{8,16},{16,24},{24,0},{1,9},{9,17},{17,25},{25,1},{2,10},{10... | collective-permute-start | bytes 589832 | tf_op jit(solution)/shard_map/ppermute | solution.py:146
  9.3 2.6 %collective-permute-start.2 = (bf16[48,2048]{1,0:T(8,128)(2,1)}, bf16[48,2048]{1,0:T(8,128)(2,1)S(1)}, u32[]{:S(2)}, u32[]{:S(2)}) collective-permute-start(bf16[48,2048]{1,0:T(8,128)(2,1)} %get-tuple-element.13), channel_id=1, source_target_pairs={{0,16},{8,24},{16,0},{24,8},{1,17},{9,25},{17,1},{25,9},{2,18},{10... | collective-permute-start | bytes 589832 | tf_op jit(solution)/shard_map/ppermute | solution.py:146
  11.9 1.3 %collective-permute-start.4 = (bf16[48,2048]{1,0:T(8,128)(2,1)}, bf16[48,2048]{1,0:T(8,128)(2,1)S(1)}, u32[]{:S(2)}, u32[]{:S(2)}) collective-permute-start(bf16[48,2048]{1,0:T(8,128)(2,1)} %get-tuple-element.14), channel_id=1, source_target_pairs={{0,24},{8,0},{16,8},{24,16},{1,25},{9,1},{17,9},{25,17},{2,26},{10... | collective-permute-start | bytes 589832 | tf_op jit(solution)/shard_map/ppermute | solution.py:146
  13.2 4.2 %collective-permute-done = bf16[48,2048]{1,0:T(8,128)(2,1)S(1)} collective-permute-done((bf16[48,2048]{1,0:T(8,128)(2,1)}, bf16[48,2048]{1,0:T(8,128)(2,1)S(1)}, u32[]{:S(2)}, u32[]{:S(2)}) %collective-permute-start) | collective-permute-done | bytes 196640 | tf_op jit(solution)/shard_map/ppermute | solution.py:146
  17.4 1.0 %constant_dynamic-update-slice_fusion = bf16[384,2048]{1,0:T(8,128)(2,1)S(1)} fusion(bf16[96,2048]{1,0:T(8,128)(2,1)} %get-tuple-element.11), kind=kLoop, calls=%fused_computation.20 | loop fusion | bytes 786432
  18.4 6.5 %collective-permute-done.2 = bf16[48,2048]{1,0:T(8,128)(2,1)S(1)} collective-permute-done((bf16[48,2048]{1,0:T(8,128)(2,1)}, bf16[48,2048]{1,0:T(8,128)(2,1)S(1)}, u32[]{:S(2)}, u32[]{:S(2)}) %collective-permute-start.2) | collective-permute-done | bytes 196640 | tf_op jit(solution)/shard_map/ppermute | solution.py:146
  25.0 0.5 collective-permute-start.5
  25.6 0.8 %collective-permute-done.3 = bf16[48,2048]{1,0:T(8,128)(2,1)S(1)} collective-permute-done((bf16[48,2048]{1,0:T(8,128)(2,1)S(1)}, bf16[48,2048]{1,0:T(8,128)(2,1)S(1)}, u32[]{:S(2)}, u32[]{:S(2)}) %collective-permute-start.3) | collective-permute-done | bytes 196640 | tf_op jit(solution)/shard_map/ppermute | solution.py:147
  26.5 0.2 collective-permute-done.5
  26.8 4.9 %fusion.2 = f32[384,1536]{1,0:T(8,128)S(1)} fusion(bf16[384,2048]{1,0:T(8,128)(2,1)S(1)} %select_dynamic-update-slice_fusion, bf16[1,2048,1536]{2,1,0:T(8,128)(2,1)} %param.11), kind=kOutput, calls=%fused_computation.2 | convolution fusion | flops 2415919104 | bytes 10223616 | tf_op jit(solution)/shard_map/dot_general | solution.py:151
  31.8 3.8 %multiply_convert_fusion.hidden_ref = bf16[384,1536]{1,0:T(8,128)(2,1)} fusion(f32[384,1536]{1,0:T(8,128)S(1)} %fusion.2, bf16[384,2048]{1,0:T(8,128)(2,1)S(1)} %select_dynamic-update-slice_fusion, bf16[1,2048,1536]{2,1,0:T(8,128)(2,1)S(1)} %bitcast.34), kind=kOutput, calls=%fused_computation.4 | convolution fusion | flops 2419458048 | bytes 11403264 | tf_op jit(solution)/shard_map/dot_general | solution.py:152
  35.5 5.0 %shard_map.75 = bf16[4,384,256]{2,1,0:T(8,128)(2,1)} custom-call(s32[1]{0:T(128)} %bitcast.6.where_ref, bf16[384,1536]{1,0:T(8,128)(2,1)} %multiply_convert_fusion.hidden_ref, bf16[1536,2048]{1,0:T(8,128)(2,1)} %bitcast.28), custom_call_target="tpu_custom_call" | custom-call | flops 1207959552 | bytes 3145728 | tf_op jit(solution)/shard_map/pallas_call | solution.py:80
  40.6 0.2 collective-permute-start.6
  40.8 5.0 %shard_map.74 = bf16[4,384,256]{2,1,0:T(8,128)(2,1)} custom-call(s32[1]{0:T(128)} %bitcast.1.where_ref, bf16[384,1536]{1,0:T(8,128)(2,1)} %multiply_convert_fusion.hidden_ref, bf16[1536,2048]{1,0:T(8,128)(2,1)} %bitcast.29), custom_call_target="tpu_custom_call" | custom-call | flops 1207959552 | bytes 3145728 | tf_op jit(solution)/shard_map/pallas_call | solution.py:80
  45.8 1.3 %convert_add_fusion = bf16[4,384,256]{2,1,0:T(8,128)(2,1)S(1)} fusion(bf16[4,384,256]{2,1,0:T(8,128)(2,1)S(1)} %collective-permute-done.6, bf16[4,384,256]{2,1,0:T(8,128)(2,1)} %shard_map.74), kind=kLoop, calls=%fused_computation.7 | loop fusion | flops 1572864 | bytes 2359296 | tf_op jit(solution)/shard_map/add | solution.py:159
  47.3 1.5 %collective-permute-start.7 = (bf16[2,384,256]{2,1,0:T(8,128)(2,1)S(1)}, bf16[2,384,256]{2,1,0:T(8,128)(2,1)S(1)}, u32[]{:S(2)}, u32[]{:S(2)}) collective-permute-start(bf16[2,384,256]{2,1,0:T(8,128)(2,1)S(1)} %dynamic-slice_bitcast_fusion), channel_id=1, source_target_pairs={{0,2},{1,5},{2,0},{3,7},{4,6},{5,1},{6,4},{7,3},{8,10},{9,13},{10,... | collective-permute-start | bytes 1179656 | tf_op jit(solution)/shard_map/ppermute | solution.py:169
  48.8 6.3 %collective-permute-done.7 = bf16[2,384,256]{2,1,0:T(8,128)(2,1)S(1)} collective-permute-done((bf16[2,384,256]{2,1,0:T(8,128)(2,1)S(1)}, bf16[2,384,256]{2,1,0:T(8,128)(2,1)S(1)}, u32[]{:S(2)}, u32[]{:S(2)}) %collective-permute-start.7) | collective-permute-done | bytes 393248 | tf_op jit(solution)/shard_map/ppermute | solution.py:169
  55.1 0.1 fusion.5
  55.3 1.5 %collective-permute-start.8 = (bf16[384,256]{1,0:T(8,128)(2,1)S(1)}, bf16[384,256]{1,0:T(8,128)(2,1)S(1)}, u32[]{:S(2)}, u32[]{:S(2)}) collective-permute-start(bf16[384,256]{1,0:T(8,128)(2,1)S(1)} %dynamic-slice_bitcast_fusion.1), channel_id=1, source_target_pairs={{0,4},{1,3},{2,6},{3,1},{4,0},{5,7},{6,2},{7,5},{8,12},{9,11},{10,... | collective-permute-start | bytes 589832 | tf_op jit(solution)/shard_map/ppermute | solution.py:169
  56.8 4.2 %collective-permute-done.8 = bf16[384,256]{1,0:T(8,128)(2,1)S(1)} collective-permute-done((bf16[384,256]{1,0:T(8,128)(2,1)S(1)}, bf16[384,256]{1,0:T(8,128)(2,1)S(1)}, u32[]{:S(2)}, u32[]{:S(2)}) %collective-permute-start.8) | collective-permute-done | bytes 196640 | tf_op jit(solution)/shard_map/ppermute | solution.py:169
  61.1 0.6 fusion.7
  61.7 3.4 %collective-permute-start.10 = (bf16[96,256]{1,0:T(8,128)(2,1)S(1)}, bf16[96,256]{1,0:T(8,128)(2,1)S(1)}, u32[]{:S(2)}, u32[]{:S(2)}) collective-permute-start(bf16[96,256]{1,0:T(8,128)(2,1)S(1)} %get-tuple-element.16), channel_id=1, source_target_pairs={{0,16},{8,24},{16,0},{24,8},{1,17},{9,25},{17,1},{25,9},{2,18},{10... | collective-permute-start | bytes 147464 | tf_op jit(solution)/shard_map/ppermute | solution.py:175
  65.1 2.9 %collective-permute-start.11 = (bf16[96,256]{1,0:T(8,128)(2,1)S(1)}, bf16[96,256]{1,0:T(8,128)(2,1)S(1)}, u32[]{:S(2)}, u32[]{:S(2)}) collective-permute-start(bf16[96,256]{1,0:T(8,128)(2,1)S(1)} %get-tuple-element.15), channel_id=1, source_target_pairs={{0,8},{8,16},{16,24},{24,0},{1,9},{9,17},{17,25},{25,1},{2,10},{10... | collective-permute-start | bytes 147464 | tf_op jit(solution)/shard_map/ppermute | solution.py:175
  68.0 0.9 %collective-permute-start.9 = (bf16[96,256]{1,0:T(8,128)(2,1)S(1)}, bf16[96,256]{1,0:T(8,128)(2,1)S(1)}, u32[]{:S(2)}, u32[]{:S(2)}) collective-permute-start(bf16[96,256]{1,0:T(8,128)(2,1)S(1)} %get-tuple-element.17), channel_id=1, source_target_pairs={{0,24},{8,0},{16,8},{24,16},{1,25},{9,1},{17,9},{25,17},{2,26},{10... | collective-permute-start | bytes 147464 | tf_op jit(solution)/shard_map/ppermute | solution.py:175
  68.9 2.1 %collective-permute-done.11.refs_3_ = bf16[96,256]{1,0:T(8,128)(2,1)S(1)} collective-permute-done((bf16[96,256]{1,0:T(8,128)(2,1)S(1)}, bf16[96,256]{1,0:T(8,128)(2,1)S(1)}, u32[]{:S(2)}, u32[]{:S(2)}) %collective-permute-start.11) | collective-permute-done | bytes 49184 | tf_op jit(solution)/shard_map/ppermute | solution.py:175
  71.0 1.1 %collective-permute-done.9.refs_1_ = bf16[96,256]{1,0:T(8,128)(2,1)S(1)} collective-permute-done((bf16[96,256]{1,0:T(8,128)(2,1)S(1)}, bf16[96,256]{1,0:T(8,128)(2,1)S(1)}, u32[]{:S(2)}, u32[]{:S(2)}) %collective-permute-start.9) | collective-permute-done | bytes 49184 | tf_op jit(solution)/shard_map/ppermute | solution.py:175
  72.1 0.6 copy-done.2
  72.7 1.9 %shard_map.76 = bf16[128,256]{1,0:T(8,128)(2,1)} custom-call(f32[128,384]{1,0:T(8,128)} %get-tuple-element.10.mix_ref, bf16[96,256]{1,0:T(8,128)(2,1)} %get-tuple-element.18.refs_0_, bf16[96,256]{1,0:T(8,128)(2,1)} %copy-done.2, bf16[96,256]{1,0:T(8,128)(2,1)} %copy-done, bf16[96,256]{1,0:T(8,128)(2,1)} %copy-done.1), custom_call_target="tpu_custom_call" | custom-call | tf_op jit(solution)/shard_map/pallas_call | solution.py:176
  (26 shorter events, 0.6 us)
Async XLA Ops:
  6.2 11.2 %collective-permute-start = (bf16[48,2048]{1,0:T(8,128)(2,1)}, bf16[48,2048]{1,0:T(8,128)(2,1)S(1)}, u32[]{:S(2)}, u32[]{:S(2)}) collective-permute-start(bf16[48,2048]{1,0:T(8,128)(2,1)} %get-tuple-element.12), channel_id=1, source_target_pairs={{0,8},{8,16},{16,24},{24,0},{1,9},{9,17},{17,25},{25,1},{2,10},{10... | collective-permute-start | bytes 589832 | tf_op jit(solution)/shard_map/ppermute | solution.py:146
  9.3 15.7 %collective-permute-start.2 = (bf16[48,2048]{1,0:T(8,128)(2,1)}, bf16[48,2048]{1,0:T(8,128)(2,1)S(1)}, u32[]{:S(2)}, u32[]{:S(2)}) collective-permute-start(bf16[48,2048]{1,0:T(8,128)(2,1)} %get-tuple-element.13), channel_id=1, source_target_pairs={{0,16},{8,24},{16,0},{24,8},{1,17},{9,25},{17,1},{25,9},{2,18},{10... | collective-permute-start | bytes 589832 | tf_op jit(solution)/shard_map/ppermute | solution.py:146
  11.9 13.1 %collective-permute-start.4 = (bf16[48,2048]{1,0:T(8,128)(2,1)}, bf16[48,2048]{1,0:T(8,128)(2,1)S(1)}, u32[]{:S(2)}, u32[]{:S(2)}) collective-permute-start(bf16[48,2048]{1,0:T(8,128)(2,1)} %get-tuple-element.14), channel_id=1, source_target_pairs={{0,24},{8,0},{16,8},{24,16},{1,25},{9,1},{17,9},{25,17},{2,26},{10... | collective-permute-start | bytes 589832 | tf_op jit(solution)/shard_map/ppermute | solution.py:146
  17.4 8.1 %collective-permute-start.1 = (bf16[48,2048]{1,0:T(8,128)(2,1)S(1)}, bf16[48,2048]{1,0:T(8,128)(2,1)S(1)}, u32[]{:S(2)}, u32[]{:S(2)}) collective-permute-start(bf16[48,2048]{1,0:T(8,128)(2,1)S(1)} %collective-permute-done), channel_id=1, source_target_pairs={{0,1},{1,0},{2,3},{3,2},{4,5},{5,4},{6,7},{7,6},{8,9},{9,8},{10,11... | collective-permute-start | bytes 589832 | tf_op jit(solution)/shard_map/ppermute | solution.py:147
  25.0 1.4 %collective-permute-start.3 = (bf16[48,2048]{1,0:T(8,128)(2,1)S(1)}, bf16[48,2048]{1,0:T(8,128)(2,1)S(1)}, u32[]{:S(2)}, u32[]{:S(2)}) collective-permute-start(bf16[48,2048]{1,0:T(8,128)(2,1)S(1)} %collective-permute-done.2), channel_id=1, source_target_pairs={{0,1},{1,0},{2,3},{3,2},{4,5},{5,4},{6,7},{7,6},{8,9},{9,8},{10,11... | collective-permute-start | bytes 589832 | tf_op jit(solution)/shard_map/ppermute | solution.py:147
  25.0 1.7 %collective-permute-start.5 = (bf16[48,2048]{1,0:T(8,128)(2,1)S(1)}, bf16[48,2048]{1,0:T(8,128)(2,1)S(1)}, u32[]{:S(2)}, u32[]{:S(2)}) collective-permute-start(bf16[48,2048]{1,0:T(8,128)(2,1)S(1)} %collective-permute-done.4), channel_id=1, source_target_pairs={{0,1},{1,0},{2,3},{3,2},{4,5},{5,4},{6,7},{7,6},{8,9},{9,8},{10,11... | collective-permute-start | bytes 589832 | tf_op jit(solution)/shard_map/ppermute | solution.py:147
  26.8 5.0 %slice-start = ((s8[6291456]{0:T(1024)(128)(4,1)}), s8[4194304]{0:T(1024)(128)(4,1)S(1)}, s32[]{:S(2)}) async-start(s8[6291456]{0:T(1024)(128)(4,1)} %bitcast.33), calls=%async_computation | async-start | bytes 8388608
  26.8 4.9 %slice-start.1 = ((s8[6291456]{0:T(1024)(128)(4,1)}), s8[2097152]{0:T(1024)(128)(4,1)S(1)}, s32[]{:S(2)}) async-start(s8[6291456]{0:T(1024)(128)(4,1)} %bitcast.33), calls=%async_computation.1 | async-start | bytes 4194304
  40.6 5.3 %collective-permute-start.6 = (bf16[4,384,256]{2,1,0:T(8,128)(2,1)}, bf16[4,384,256]{2,1,0:T(8,128)(2,1)S(1)}, u32[]{:S(2)}, u32[]{:S(2)}) collective-permute-start(bf16[4,384,256]{2,1,0:T(8,128)(2,1)} %shard_map.75), channel_id=1, source_target_pairs={{0,1},{1,0},{2,3},{3,2},{4,5},{5,4},{6,7},{7,6},{8,9},{9,8},{10,11... | collective-permute-start | bytes 2359304 | tf_op jit(solution)/shard_map/ppermute | solution.py:156
  47.3 7.8 %collective-permute-start.7 = (bf16[2,384,256]{2,1,0:T(8,128)(2,1)S(1)}, bf16[2,384,256]{2,1,0:T(8,128)(2,1)S(1)}, u32[]{:S(2)}, u32[]{:S(2)}) collective-permute-start(bf16[2,384,256]{2,1,0:T(8,128)(2,1)S(1)} %dynamic-slice_bitcast_fusion), channel_id=1, source_target_pairs={{0,2},{1,5},{2,0},{3,7},{4,6},{5,1},{6,4},{7,3},{8,10},{9,13},{10,... | collective-permute-start | bytes 1179656 | tf_op jit(solution)/shard_map/ppermute | solution.py:169
  55.3 5.7 %collective-permute-start.8 = (bf16[384,256]{1,0:T(8,128)(2,1)S(1)}, bf16[384,256]{1,0:T(8,128)(2,1)S(1)}, u32[]{:S(2)}, u32[]{:S(2)}) collective-permute-start(bf16[384,256]{1,0:T(8,128)(2,1)S(1)} %dynamic-slice_bitcast_fusion.1), channel_id=1, source_target_pairs={{0,4},{1,3},{2,6},{3,1},{4,0},{5,7},{6,2},{7,5},{8,12},{9,11},{10,... | collective-permute-start | bytes 589832 | tf_op jit(solution)/shard_map/ppermute | solution.py:169
  61.7 7.2 %collective-permute-start.10 = (bf16[96,256]{1,0:T(8,128)(2,1)S(1)}, bf16[96,256]{1,0:T(8,128)(2,1)S(1)}, u32[]{:S(2)}, u32[]{:S(2)}) collective-permute-start(bf16[96,256]{1,0:T(8,128)(2,1)S(1)} %get-tuple-element.16), channel_id=1, source_target_pairs={{0,16},{8,24},{16,0},{24,8},{1,17},{9,25},{17,1},{25,9},{2,18},{10... | collective-permute-start | bytes 147464 | tf_op jit(solution)/shard_map/ppermute | solution.py:175
  65.1 5.9 %collective-permute-start.11 = (bf16[96,256]{1,0:T(8,128)(2,1)S(1)}, bf16[96,256]{1,0:T(8,128)(2,1)S(1)}, u32[]{:S(2)}, u32[]{:S(2)}) collective-permute-start(bf16[96,256]{1,0:T(8,128)(2,1)S(1)} %get-tuple-element.15), channel_id=1, source_target_pairs={{0,8},{8,16},{16,24},{24,0},{1,9},{9,17},{17,25},{25,1},{2,10},{10... | collective-permute-start | bytes 147464 | tf_op jit(solution)/shard_map/ppermute | solution.py:175
  68.0 4.1 %collective-permute-start.9 = (bf16[96,256]{1,0:T(8,128)(2,1)S(1)}, bf16[96,256]{1,0:T(8,128)(2,1)S(1)}, u32[]{:S(2)}, u32[]{:S(2)}) collective-permute-start(bf16[96,256]{1,0:T(8,128)(2,1)S(1)} %get-tuple-element.17), channel_id=1, source_target_pairs={{0,24},{8,0},{16,8},{24,16},{1,25},{9,1},{17,9},{25,17},{2,26},{10... | collective-permute-start | bytes 147464 | tf_op jit(solution)/shard_map/ppermute | solution.py:175
  68.9 3.2 %copy-start = (bf16[96,256]{1,0:T(8,128)(2,1)}, bf16[96,256]{1,0:T(8,128)(2,1)S(1)}, u32[]{:S(2)}) copy-start(bf16[96,256]{1,0:T(8,128)(2,1)S(1)} %collective-permute-done.10.refs_2_) | copy-start | bytes 147460
  71.0 1.1 %copy-start.1 = (bf16[96,256]{1,0:T(8,128)(2,1)}, bf16[96,256]{1,0:T(8,128)(2,1)S(1)}, u32[]{:S(2)}) copy-start(bf16[96,256]{1,0:T(8,128)(2,1)S(1)} %collective-permute-done.11.refs_3_) | copy-start | bytes 147460
  72.1 0.6 copy-start.2
